TPU v7x, 32 devices: a whole 2x2x4 slice. The times are simulated.
32 devices in a mesh: pp: 4 (over y, x), tp: 8 (over z, core).
Axes of the slice: x: 2, y: 2, z: 4, core: 2. Of those that a mesh axis runs over, the one named last changes fastest.
Arguments:
- entry_stream_rows: bfloat16 [256, 2048], P('pp', 'tp'), may hold values from -21 to 21
- layer_rescale_factor: float32 [4, 2048], P('pp'), may hold values from 0.1 to 1.9
- probe_projection: bfloat16 [4, 2048, 2048], P('pp', 'tp'), may hold values from -0.125 to 0.125
- retention_projection: bfloat16 [4, 2048, 2048], P('pp', 'tp'), may hold values from -0.125 to 0.125
- candidate_projection: bfloat16 [4, 2048, 2048], P('pp', 'tp'), may hold values from -0.125 to 0.125
- emission_filter_matrix: bfloat16 [4, 2048, 2048], P('pp', 'tp'), may hold values from -0.125 to 0.125
- retention_minimum: float32 [4, 2048], P('pp', 'tp'), may hold values from 0.88 to 0.9921875
- decay_spike: float32 [4, 128, 32], P('pp', None, 'tp'), may hold values from -2.1 to 0
- per_group_scale: float32 [4, 64], P('pp'), may hold values from 0.1 to 1.9
Outputs:
- outputs: bfloat16 [256, 2048], P('pp', 'tp')
All inputs are finite; a program needn't handle non-finite values.
Results may differ from a plain program's by a relative error of at most 0.03.
Values may be sent and summed in bfloat16 or wider, within the bound.
A program may use at most 64 MiB of HBM per device.

v0:
```python
import jax
import jax.numpy as jnp
from jax import lax
from jax.sharding import PartitionSpec as P

HEAD = 64
SEG = 64


EPSILON = 1e-06
HIGHEST = lax.Precision.HIGHEST


def shifted(array, axis, by):
    devices = lax.axis_size(axis)
    pairs = [(i, i + by) for i in range(devices) if 0 <= i + by < devices]
    return lax.ppermute(array, axis, pairs)


def spread(value, axis, source):
    kept = jnp.where(lax.axis_index(axis) == source, value, 0).astype(value.dtype)
    return lax.psum(kept, axis)


def segment_scan(queries, key_in, log_forget, values, memory):
    head_count = queries.shape[0]
    length = queries.shape[1]
    blocks_count = length // SEG

    def split_blocks(tensor):
        return tensor.reshape(head_count, blocks_count, SEG, tensor.shape[-1]).transpose(1, 0, 2, 3)

    lower_mask = jnp.tril(jnp.ones((SEG, SEG), dtype=bool))[None]

    def one_block(memory_in, pieces):
        block_query, block_key, block_forget, block_value = pieces
        running = jnp.cumsum(block_forget, axis=1)
        query_scaled = block_query * jnp.exp(running)
        key_scaled = block_key * jnp.exp(-running)
        scores = jnp.einsum("hid,hjd->hij", query_scaled, key_scaled, precision=HIGHEST)
        scores = jnp.where(lower_mask, scores, 0.0)
        mixed_out = jnp.einsum("hij,hjv->hiv", scores, block_value, precision=HIGHEST)
        mixed_out = mixed_out + jnp.einsum(
            "hid,hdv->hiv", query_scaled, memory_in, precision=HIGHEST
        )
        ending = running[:, -1:, :]
        carried_in = jnp.einsum(
            "hjd,hjv->hdv", block_key * jnp.exp(ending - running), block_value, precision=HIGHEST
        )
        memory_out = jnp.exp(ending[:, 0, :])[:, :, None] * memory_in + carried_in
        return (memory_out, mixed_out)

    memory, mixed_out = lax.scan(
        one_block,
        memory,
        (
            split_blocks(queries),
            split_blocks(key_in),
            split_blocks(log_forget),
            split_blocks(values),
        ),
    )
    return (mixed_out.transpose(1, 0, 2, 3).reshape(head_count, length, values.shape[-1]), memory)


def head_norm(mixed_out, channel_gain):
    return (
        mixed_out
        * lax.rsqrt(jnp.mean(mixed_out * mixed_out, axis=-1, keepdims=True) + EPSILON)
        * channel_gain
    )


def shards(
    entry_stream_rows,
    layer_rescale_factor,
    probe_projection,
    retention_projection,
    candidate_projection,
    emission_filter_matrix,
    retention_minimum,
    decay_spike,
    per_group_scale,
):
    sections = lax.axis_size("pp")
    layer_ordinal = lax.axis_index("pp")
    own_rows = entry_stream_rows.shape[0]
    seq_len = 2 * own_rows
    columns = entry_stream_rows.shape[1]
    head_here = columns // HEAD
    model_width = layer_rescale_factor.shape[1]
    micro_count = sections // 2
    per_sequence = seq_len // seq_len
    unit_count = micro_count * per_sequence
    total_steps = unit_count + sections - 1
    entering = lax.all_gather(entry_stream_rows, "pp", axis=0, tiled=True)
    weights = jnp.concatenate(
        [
            probe_projection[0],
            retention_projection[0],
            candidate_projection[0],
            emission_filter_matrix[0],
        ],
        axis=0,
    )
    input_gain = layer_rescale_factor[0]
    lower_edge = retention_minimum[0].reshape(head_here, 1, HEAD)
    spike_collection = decay_spike[0].T
    out_gain = per_group_scale[0]

    def add_piece(piece_in):
        wide_piece = piece_in.astype(jnp.float32)
        scaled = (wide_piece * input_gain[None, :]).astype(jnp.bfloat16)
        product = lax.dot_general(
            scaled, weights, (((1,), (1,)), ((), ())), preferred_element_type=jnp.float32
        )
        return (product, jnp.sum(wide_piece * wide_piece, axis=1))

    def one_step(step_index, carried):
        incoming, memory, finished = carried
        unit_index = step_index - layer_ordinal
        first_slot = jnp.clip(step_index, 0, unit_count - 1)
        fresh_rows = lax.dynamic_slice_in_dim(entering, first_slot * seq_len, seq_len, 0)
        current = jnp.where(layer_ordinal == 0, fresh_rows, incoming)
        projected, squares = add_piece(lax.all_gather(current, "tp", axis=1, tiled=True))
        inverse = lax.rsqrt(squares / model_width + EPSILON)[:, None]
        projected = projected * inverse

        def per_head(role_index):
            picked = projected[:, role_index * columns : (role_index + 1) * columns]
            return picked.reshape(seq_len, head_here, HEAD).transpose(1, 0, 2)

        query_pre = per_head(0)
        forget_pre = per_head(1)
        input_pre = per_head(2)
        gate_pre = per_head(3)
        offset = unit_index % per_sequence * seq_len
        current_surge = spike_collection[:, :, None]
        log_forget = (
            jnp.logaddexp(
                jnp.log(lower_edge), jnp.log1p(-lower_edge) + jax.nn.log_sigmoid(forget_pre)
            )
            + current_surge
        )
        key_in = (1.0 - lower_edge) * jax.nn.sigmoid(-forget_pre)
        queries = jax.nn.silu(query_pre)
        memory = jnp.where(offset == 0, jnp.zeros_like(memory), memory)
        mixed_out, memory = segment_scan(queries, key_in, log_forget, input_pre, memory)
        branch = head_norm(mixed_out, out_gain) * jax.nn.silu(gate_pre)
        branch = branch.transpose(1, 0, 2).reshape(seq_len, columns)
        result = (current.astype(jnp.float32) + branch).astype(jnp.bfloat16)
        passed = shifted(result, "pp", 1)
        out_slot = jnp.clip(unit_index, 0, unit_count - 1)
        write_here = (layer_ordinal == sections - 1) & (unit_index >= 0) & (unit_index < unit_count)
        updated = lax.dynamic_update_slice_in_dim(finished, result, out_slot * seq_len, 0)
        finished = jnp.where(write_here, updated, finished)
        return (passed, memory, finished)

    start_state = (
        jnp.zeros((seq_len, columns), jnp.bfloat16),
        jnp.zeros((head_here, HEAD, HEAD), jnp.float32),
        jnp.zeros((unit_count * seq_len, columns), jnp.bfloat16),
    )
    carried_out = lax.fori_loop(0, total_steps, one_step, start_state)
    everything = spread(carried_out[2], "pp", sections - 1)
    return lax.dynamic_slice_in_dim(everything, layer_ordinal * own_rows, own_rows, 0)


def solution(mesh):
    in_specs = (
        P("pp", "tp"),
        P("pp", None),
        P("pp", "tp", None),
        P("pp", "tp", None),
        P("pp", "tp", None),
        P("pp", "tp", None),
        P("pp", "tp"),
        P("pp", None, "tp"),
        P("pp", None),
    )
    out_specs = P("pp", "tp")
    return jax.shard_map(shards, mesh=mesh, in_specs=in_specs, out_specs=out_specs, check_vma=False)
```

profile of v0, /device:TPU:7, one launch (start us, length us, event | category | flops | bytes accessed | tf_op | source)
XLA Modules:
  0.0 242.3 jit_solution(12410205212231642517)
XLA Ops:
  8.6 5.9 %all_gather.14 = bf16[256,256]{1,0:T(8,128)(2,1)S(1)} all-gather(bf16[64,256]{1,0:T(8,128)(2,1)} %param.13), channel_id=1, replica_groups=mesh['pp'=4,'tp'=8] {'pp'}, dimensions={0}, use_global_device_ids=true | all-gather | bytes 163840 | tf_op jit(solution)/shard_map/all_gather | solution.py:96
  14.6 3.7 %pad_maximum_fusion = bf16[1024,2048]{1,0:T(8,128)(2,1)} fusion(bf16[256,2048]{1,0:T(8,128)(2,1)} %bitcast.150, bf16[256,2048]{1,0:T(8,128)(2,1)} %bitcast.151, bf16[256,2048]{1,0:T(8,128)(2,1)} %bitcast.152, bf16[256,2048]{1,0:T(8,128)(2,1)} %bitcast.153), kind=kLoop, calls=%fused_computation.50 | loop fusion | flops 16777216 | bytes 8388608 | tf_op jit(solution)/shard_map/concatenate | solution.py:97
  18.3 171.7 %while.59 = (s32[]{:T(128)}, bf16[128,256]{0,1:T(8,128)(2,1)S(1)}, bf16[256,256]{1,0:T(8,128)(2,1)S(1)}, pred[]{:T(512)}, bf16[256,256]{1,0:T(8,128)(2,1)S(1)}, ...) while((s32[]{:T(128)}, bf16[128,256]{0,1:T(8,128)(2,1)S(1)}, ...), condition=%wide.region_6.7_spmd, body=%wide.region_0.6_spmd.sunk | while | flops 591418240 | bytes 15908739 | solution.py:164
  18.6 17.4 %all_gather.16 = bf16[128,2048]{0,1:T(8,128)(2,1)S(1)} all-gather(bf16[128,256]{0,1:T(8,128)(2,1)S(1)} %broadcast_select_fusion.5), channel_id=1, replica_groups=mesh['pp'=4,'tp'=8] {'tp'}, dimensions={1}, use_global_device_ids=true | all-gather | bytes 589824 | tf_op jit(solution)/shard_map/while/body/eval_jaxpr/all_gather | solution.py:125
  36.3 4.2 %convolution_multiply_fusion.2 = f32[128,1024]{1,0:T(8,128)S(1)} fusion(bf16[1024,2048]{1,0:T(8,128)(2,1)} %get-tuple-element.759, bf16[128,2048]{0,1:T(8,128)(2,1)S(1)} %all_gather.16, f32[2048]{0:T(1024)S(1)} %bitcast.154, f32[128]{0:T(128)S(1)} %add_rsqrt_fusion.4), kind=kOutput, calls=%fused_computation.26.clone.1 | convolution fusion | flops 537788416 | bytes 5251584 | tf_op jit(solution)/shard_map/while/body/eval_jaxpr/dot_general | solution.py:114
  42.0 5.0 %while.60 = (s32[]{:T(128)}, f32[4,64,64]{2,1,0:T(8,128)S(1)}, f32[2,4,64,64]{3,2,1,0:T(8,128)S(1)}, f32[2,4,64,64]{2,0,3,1:T(2,128)S(1)}, f32[2,4,64,64]{2,0,3,...) while((s32[]{:T(128)}, f32[4,64,64]{2,1,0:T(8,128)S(1)}, ...), condition=%wide.region_4.4_spmd.clone, body=%wide.region_2.3_spmd.clone.sunk | while | flops 51564544 | bytes 2504832 | solution.py:53
  49.5 3.9 %collective-permute-done = bf16[128,256]{0,1:T(8,128)(2,1)S(1)} collective-permute-done((bf16[128,256]{0,1:T(8,128)(2,1)S(1)}, bf16[128,256]{0,1:T(8,128)(2,1)S(1)}, u32[]{:S(2)}, u32[]{:S(2)}) %collective-permute-start) | collective-permute-done | bytes 65568 | tf_op jit(solution)/shard_map/while/body/eval_jaxpr/ppermute | solution.py:17
  53.6 15.6 %all_gather.16 = bf16[128,2048]{0,1:T(8,128)(2,1)S(1)} all-gather(bf16[128,256]{0,1:T(8,128)(2,1)S(1)} %broadcast_select_fusion.5), channel_id=1, replica_groups=mesh['pp'=4,'tp'=8] {'tp'}, dimensions={1}, use_global_device_ids=true | all-gather | bytes 589824 | tf_op jit(solution)/shard_map/while/body/eval_jaxpr/all_gather | solution.py:125
  69.4 4.2 %convolution_multiply_fusion.2 = f32[128,1024]{1,0:T(8,128)S(1)} fusion(bf16[1024,2048]{1,0:T(8,128)(2,1)} %get-tuple-element.759, bf16[128,2048]{0,1:T(8,128)(2,1)S(1)} %all_gather.16, f32[2048]{0:T(1024)S(1)} %bitcast.154, f32[128]{0:T(128)S(1)} %add_rsqrt_fusion.4), kind=kOutput, calls=%fused_computation.26.clone.1 | convolution fusion | flops 537788416 | bytes 5251584 | tf_op jit(solution)/shard_map/while/body/eval_jaxpr/dot_general | solution.py:114
  75.2 5.0 %while.60 = (s32[]{:T(128)}, f32[4,64,64]{2,1,0:T(8,128)S(1)}, f32[2,4,64,64]{3,2,1,0:T(8,128)S(1)}, f32[2,4,64,64]{2,0,3,1:T(2,128)S(1)}, f32[2,4,64,64]{2,0,3,...) while((s32[]{:T(128)}, f32[4,64,64]{2,1,0:T(8,128)S(1)}, ...), condition=%wide.region_4.4_spmd.clone, body=%wide.region_2.3_spmd.clone.sunk | while | flops 51564544 | bytes 2504832 | solution.py:53
  82.6 4.7 %collective-permute-done = bf16[128,256]{0,1:T(8,128)(2,1)S(1)} collective-permute-done((bf16[128,256]{0,1:T(8,128)(2,1)S(1)}, bf16[128,256]{0,1:T(8,128)(2,1)S(1)}, u32[]{:S(2)}, u32[]{:S(2)}) %collective-permute-start) | collective-permute-done | bytes 65568 | tf_op jit(solution)/shard_map/while/body/eval_jaxpr/ppermute | solution.py:17
  87.4 15.6 %all_gather.16 = bf16[128,2048]{0,1:T(8,128)(2,1)S(1)} all-gather(bf16[128,256]{0,1:T(8,128)(2,1)S(1)} %broadcast_select_fusion.5), channel_id=1, replica_groups=mesh['pp'=4,'tp'=8] {'tp'}, dimensions={1}, use_global_device_ids=true | all-gather | bytes 589824 | tf_op jit(solution)/shard_map/while/body/eval_jaxpr/all_gather | solution.py:125
  103.3 4.2 %convolution_multiply_fusion.2 = f32[128,1024]{1,0:T(8,128)S(1)} fusion(bf16[1024,2048]{1,0:T(8,128)(2,1)} %get-tuple-element.759, bf16[128,2048]{0,1:T(8,128)(2,1)S(1)} %all_gather.16, f32[2048]{0:T(1024)S(1)} %bitcast.154, f32[128]{0:T(128)S(1)} %add_rsqrt_fusion.4), kind=kOutput, calls=%fused_computation.26.clone.1 | convolution fusion | flops 537788416 | bytes 5251584 | tf_op jit(solution)/shard_map/while/body/eval_jaxpr/dot_general | solution.py:114
  109.1 5.0 %while.60 = (s32[]{:T(128)}, f32[4,64,64]{2,1,0:T(8,128)S(1)}, f32[2,4,64,64]{3,2,1,0:T(8,128)S(1)}, f32[2,4,64,64]{2,0,3,1:T(2,128)S(1)}, f32[2,4,64,64]{2,0,3,...) while((s32[]{:T(128)}, f32[4,64,64]{2,1,0:T(8,128)S(1)}, ...), condition=%wide.region_4.4_spmd.clone, body=%wide.region_2.3_spmd.clone.sunk | while | flops 51564544 | bytes 2504832 | solution.py:53
  116.5 5.1 %collective-permute-done = bf16[128,256]{0,1:T(8,128)(2,1)S(1)} collective-permute-done((bf16[128,256]{0,1:T(8,128)(2,1)S(1)}, bf16[128,256]{0,1:T(8,128)(2,1)S(1)}, u32[]{:S(2)}, u32[]{:S(2)}) %collective-permute-start) | collective-permute-done | bytes 65568 | tf_op jit(solution)/shard_map/while/body/eval_jaxpr/ppermute | solution.py:17
  121.7 15.6 %all_gather.16 = bf16[128,2048]{0,1:T(8,128)(2,1)S(1)} all-gather(bf16[128,256]{0,1:T(8,128)(2,1)S(1)} %broadcast_select_fusion.5), channel_id=1, replica_groups=mesh['pp'=4,'tp'=8] {'tp'}, dimensions={1}, use_global_device_ids=true | all-gather | bytes 589824 | tf_op jit(solution)/shard_map/while/body/eval_jaxpr/all_gather | solution.py:125
  137.6 4.2 %convolution_multiply_fusion.2 = f32[128,1024]{1,0:T(8,128)S(1)} fusion(bf16[1024,2048]{1,0:T(8,128)(2,1)} %get-tuple-element.759, bf16[128,2048]{0,1:T(8,128)(2,1)S(1)} %all_gather.16, f32[2048]{0:T(1024)S(1)} %bitcast.154, f32[128]{0:T(128)S(1)} %add_rsqrt_fusion.4), kind=kOutput, calls=%fused_computation.26.clone.1 | convolution fusion | flops 537788416 | bytes 5251584 | tf_op jit(solution)/shard_map/while/body/eval_jaxpr/dot_general | solution.py:114
  143.4 5.0 %while.60 = (s32[]{:T(128)}, f32[4,64,64]{2,1,0:T(8,128)S(1)}, f32[2,4,64,64]{3,2,1,0:T(8,128)S(1)}, f32[2,4,64,64]{2,0,3,1:T(2,128)S(1)}, f32[2,4,64,64]{2,0,3,...) while((s32[]{:T(128)}, f32[4,64,64]{2,1,0:T(8,128)S(1)}, ...), condition=%wide.region_4.4_spmd.clone, body=%wide.region_2.3_spmd.clone.sunk | while | flops 51564544 | bytes 2504832 | solution.py:53
  150.8 5.0 %collective-permute-done = bf16[128,256]{0,1:T(8,128)(2,1)S(1)} collective-permute-done((bf16[128,256]{0,1:T(8,128)(2,1)S(1)}, bf16[128,256]{0,1:T(8,128)(2,1)S(1)}, u32[]{:S(2)}, u32[]{:S(2)}) %collective-permute-start) | collective-permute-done | bytes 65568 | tf_op jit(solution)/shard_map/while/body/eval_jaxpr/ppermute | solution.py:17
  156.0 15.6 %all_gather.16 = bf16[128,2048]{0,1:T(8,128)(2,1)S(1)} all-gather(bf16[128,256]{0,1:T(8,128)(2,1)S(1)} %broadcast_select_fusion.5), channel_id=1, replica_groups=mesh['pp'=4,'tp'=8] {'tp'}, dimensions={1}, use_global_device_ids=true | all-gather | bytes 589824 | tf_op jit(solution)/shard_map/while/body/eval_jaxpr/all_gather | solution.py:125
  171.9 4.2 %convolution_multiply_fusion.2 = f32[128,1024]{1,0:T(8,128)S(1)} fusion(bf16[1024,2048]{1,0:T(8,128)(2,1)} %get-tuple-element.759, bf16[128,2048]{0,1:T(8,128)(2,1)S(1)} %all_gather.16, f32[2048]{0:T(1024)S(1)} %bitcast.154, f32[128]{0:T(128)S(1)} %add_rsqrt_fusion.4), kind=kOutput, calls=%fused_computation.26.clone.1 | convolution fusion | flops 537788416 | bytes 5251584 | tf_op jit(solution)/shard_map/while/body/eval_jaxpr/dot_general | solution.py:114
  177.6 5.0 %while.60 = (s32[]{:T(128)}, f32[4,64,64]{2,1,0:T(8,128)S(1)}, f32[2,4,64,64]{3,2,1,0:T(8,128)S(1)}, f32[2,4,64,64]{2,0,3,1:T(2,128)S(1)}, f32[2,4,64,64]{2,0,3,...) while((s32[]{:T(128)}, f32[4,64,64]{2,1,0:T(8,128)S(1)}, ...), condition=%wide.region_4.4_spmd.clone, body=%wide.region_2.3_spmd.clone.sunk | while | flops 51564544 | bytes 2504832 | solution.py:53
  185.1 5.0 %collective-permute-done = bf16[128,256]{0,1:T(8,128)(2,1)S(1)} collective-permute-done((bf16[128,256]{0,1:T(8,128)(2,1)S(1)}, bf16[128,256]{0,1:T(8,128)(2,1)S(1)}, u32[]{:S(2)}, u32[]{:S(2)}) %collective-permute-start) | collective-permute-done | bytes 65568 | tf_op jit(solution)/shard_map/while/body/eval_jaxpr/ppermute | solution.py:17
  190.8 43.4 %all-reduce.2.cloned.1.call-done = bf16[256,256]{1,0:T(8,128)(2,1)} async-done(((bf16[256,256]{1,0:T(8,128)(2,1)}), bf16[256,256]{1,0:T(8,128)(2,1)}) %all-reduce.2.cloned.1.call-update) | async-done | bytes 131088 | tf_op jit(solution)/shard_map/psum | solution.py:22
  (316 shorter events, 49.3 us)
Async XLA Ops:
  6.5 227.6 %all-reduce.2.cloned.1.call-start = ((), (), s32[]{:S(2)}) async-start(), calls=%async_computation | async-start | bytes 262144 | tf_op jit(solution)/shard_map/psum | solution.py:22
  14.5 3.8 %copy-start = (f32[1,2048]{1,0:T(1,128)S(1)}, f32[1,2048]{1,0:T(1,128)}, u32[]{:S(2)}) copy-start(f32[1,2048]{1,0:T(1,128)} %param.14) | copy-start | bytes 24580
  14.5 3.8 %copy-start.1 = (f32[1,128,4]{1,2,0:T(4,128)S(1)}, f32[1,128,4]{1,2,0:T(4,128)}, u32[]{:S(2)}) copy-start(f32[1,128,4]{1,2,0:T(4,128)} %param.20) | copy-start | bytes 6148
  14.6 3.8 %copy-start.2 = (f32[1,64]{1,0:T(1,128)S(1)}, f32[1,64]{1,0:T(1,128)}, u32[]{:S(2)}) copy-start(f32[1,64]{1,0:T(1,128)} %param.21) | copy-start | bytes 772
  48.0 5.4 %collective-permute-start = (bf16[128,256]{0,1:T(8,128)(2,1)S(1)}, bf16[128,256]{0,1:T(8,128)(2,1)S(1)}, u32[]{:S(2)}, u32[]{:S(2)}) collective-permute-start(bf16[128,256]{0,1:T(8,128)(2,1)S(1)} %get-tuple-element.665), channel_id=1, source_target_pairs={{0,8},{8,16},{16,24},{1,9},{9,17},{17,25},{2,10},{10,18},{18,26},{... | collective-permute-start | bytes 196616 | tf_op jit(solution)/shard_map/while/body/eval_jaxpr/ppermute | solution.py:17
  81.2 6.1 %collective-permute-start = (bf16[128,256]{0,1:T(8,128)(2,1)S(1)}, bf16[128,256]{0,1:T(8,128)(2,1)S(1)}, u32[]{:S(2)}, u32[]{:S(2)}) collective-permute-start(bf16[128,256]{0,1:T(8,128)(2,1)S(1)} %get-tuple-element.665), channel_id=1, source_target_pairs={{0,8},{8,16},{16,24},{1,9},{9,17},{17,25},{2,10},{10,18},{18,26},{... | collective-permute-start | bytes 196616 | tf_op jit(solution)/shard_map/while/body/eval_jaxpr/ppermute | solution.py:17
  115.1 6.5 %collective-permute-start = (bf16[128,256]{0,1:T(8,128)(2,1)S(1)}, bf16[128,256]{0,1:T(8,128)(2,1)S(1)}, u32[]{:S(2)}, u32[]{:S(2)}) collective-permute-start(bf16[128,256]{0,1:T(8,128)(2,1)S(1)} %get-tuple-element.665), channel_id=1, source_target_pairs={{0,8},{8,16},{16,24},{1,9},{9,17},{17,25},{2,10},{10,18},{18,26},{... | collective-permute-start | bytes 196616 | tf_op jit(solution)/shard_map/while/body/eval_jaxpr/ppermute | solution.py:17
  149.3 6.5 %collective-permute-start = (bf16[128,256]{0,1:T(8,128)(2,1)S(1)}, bf16[128,256]{0,1:T(8,128)(2,1)S(1)}, u32[]{:S(2)}, u32[]{:S(2)}) collective-permute-start(bf16[128,256]{0,1:T(8,128)(2,1)S(1)} %get-tuple-element.665), channel_id=1, source_target_pairs={{0,8},{8,16},{16,24},{1,9},{9,17},{17,25},{2,10},{10,18},{18,26},{... | collective-permute-start | bytes 196616 | tf_op jit(solution)/shard_map/while/body/eval_jaxpr/ppermute | solution.py:17
  183.6 6.5 %collective-permute-start = (bf16[128,256]{0,1:T(8,128)(2,1)S(1)}, bf16[128,256]{0,1:T(8,128)(2,1)S(1)}, u32[]{:S(2)}, u32[]{:S(2)}) collective-permute-start(bf16[128,256]{0,1:T(8,128)(2,1)S(1)} %get-tuple-element.665), channel_id=1, source_target_pairs={{0,8},{8,16},{16,24},{1,9},{9,17},{17,25},{2,10},{10,18},{18,26},{... | collective-permute-start | bytes 196616 | tf_op jit(solution)/shard_map/while/body/eval_jaxpr/ppermute | solution.py:17
Sparse Core Ops, SparseCore 0:
  190.9 43.1 all-reduce.1
where the time goes:
time: 246 us; the launch traced here: 242 us
  blocking collectives  85.7 us (35%)
  waiting for transfers between devices  67.1 us (27%)
  matrix products  34.7 us (14%)
  local copies, waits for them, and re-layouts  20.5 us (8%)
  between operations  13.4 us (5%)
  other arithmetic  12.1 us (5%)
  starting transfers between devices  6.46 us (3%)
    all_gather x5, blocking collectives, one_step(): lax.all_gather(current, 'tp', axis=1, tiled=True)  79.7 us
    psum x1, waiting for transfers between devices, spread(): return lax.psum(kept, axis)  43.4 us
    ppermute x5, waiting for transfers between devices, shifted(): return lax.ppermute(array, axis, pairs)  23.8 us
    dot_general x5, matrix products, add_piece(): lax.dot_general(scaled, weights, (((1,), (1,)), ((), ())), preferred_elem...  20.8 us
    dynamic_slice x50, local copies, waits for them, and re-layouts, segment_scan(): lax.scan(one_block, memory, (split_blocks(queries), split_blocks(key_in),...  8.32 us
    ppermute x5, starting transfers between devices, shifted(): return lax.ppermute(array, axis, pairs)  6.46 us
    all_gather x1, blocking collectives, shards(): entering = lax.all_gather(entry_stream_rows, 'pp', axis=0, tiled=True)  5.93 us
  transfers between devices with their start and end apart: 6, of which 6 were waited for; matrix products, arithmetic and copies ran while one was open for 0% of the time, Pallas kernels for 0%

commit v1 on v0

v1 whole, which is shorter than its diff:
```python
import functools

import jax
import jax.numpy as jnp
from jax import lax
from jax.experimental import pallas as pl
from jax.experimental.pallas import tpu as pltpu
from jax.sharding import PartitionSpec as P

HEAD = 64
EPSILON = 1e-06
F32 = jnp.float32
BF16 = jnp.bfloat16
NT = (((1,), (1,)), ((), ()))
NN = (((1,), (0,)), ((), ()))
TN = (((0,), (0,)), ((), ()))


def mm(a, b, dims):
    return lax.dot_general(a, b, dims, preferred_element_type=F32)


def sigmoid(v):
    return 1.0 / (1.0 + jnp.exp(-v))


def kernel(
    stages,
    lanes_axis,
    x_ref,
    gain_ref,
    wq_ref,
    wf_ref,
    wi_ref,
    wg_ref,
    low_ref,
    spike_ref,
    scale_ref,
    out_ref,
    weights,
    buf,
    res,
    spikes,
    state,
    w_sem,
    in_send,
    local_sem,
    direct_sem,
    forward_sem,
    send_sem,
    forward_send,
    out_sem,
):
    rows, cols = x_ref.shape
    heads = cols // HEAD
    width = gain_ref.shape[1]
    chips = lanes_axis // 2
    chunks = stages
    stage = lax.axis_index("pp")
    lane = lax.axis_index("tp")
    core = lax.rem(lane, 2)
    z = lane // 2
    partner = z * 2 + (1 - core)

    loads = []
    for role, ref in enumerate((wq_ref, wf_ref, wi_ref, wg_ref)):
        load = pltpu.make_async_copy(
            ref.at[0], weights.at[pl.ds(role * cols, cols)], w_sem.at[role]
        )
        load.start()
        loads.append(load)

    def to_first(far):
        target = lax.rem(z + far, chips) * 2 + core
        return pltpu.make_async_remote_copy(
            src_ref=x_ref,
            dst_ref=buf.at[stage, core, z],
            send_sem=in_send.at[far],
            recv_sem=direct_sem.at[stage],
            device_id={"pp": 0, "tp": target},
            device_id_type=pl.DeviceIdType.MESH,
        )

    own_copy = pltpu.make_async_copy(x_ref, buf.at[stage, core, z], direct_sem.at[stage])
    for far in range(1, chips):
        to_first(far).start()

    @pl.when(stage != 0)
    def _():
        to_first(0).start()

    @pl.when(stage == 0)
    def _():
        own_copy.start()

    head_of_lane = lax.broadcasted_iota(jnp.int32, (rows, cols), 1) // HEAD
    for part in range(2):
        piece = spike_ref[0, :, part * rows : (part + 1) * rows].T
        wide = jnp.zeros((rows, cols), F32)
        for h in range(heads):
            wide = jnp.where(head_of_lane == h, piece[:, h : h + 1], wide)
        spikes[part] = wide

    tri_row = lax.broadcasted_iota(jnp.int32, (rows, rows), 0)
    tri_col = lax.broadcasted_iota(jnp.int32, (rows, rows), 1)
    tril = tri_row >= tri_col
    tril_ones = jnp.where(tril, 1.0, 0.0).astype(BF16)
    tall_row = lax.rem(lax.broadcasted_iota(jnp.int32, (heads * rows, rows), 0), rows)
    tall_col = lax.broadcasted_iota(jnp.int32, (heads * rows, rows), 1)
    tall_mask = tall_row >= tall_col
    sq_row = lax.broadcasted_iota(jnp.int32, (cols, cols), 0) // HEAD
    sq_col = lax.broadcasted_iota(jnp.int32, (cols, cols), 1) // HEAD
    same_head = sq_row == sq_col
    mean_ones = jnp.where(same_head, 1.0 / HEAD, 0.0).astype(BF16)
    gain = gain_ref[...]
    span = 1.0 - low_ref[...]
    out_gain = jnp.concatenate([scale_ref[...]] * heads, axis=1)

    for load in loads:
        load.wait()

    def whole_wait(c, which, sem):
        half = buf.at[c, which]
        pltpu.make_async_copy(half, half, sem).wait()

    def forward(c):
        half = buf.at[c, core]
        return pltpu.make_async_remote_copy(
            src_ref=half,
            dst_ref=half,
            send_sem=forward_send.at[c],
            recv_sem=forward_sem.at[c],
            device_id={"pp": stage, "tp": partner},
            device_id_type=pl.DeviceIdType.MESH,
        )

    def to_next(c, far):
        target = lax.rem(z + far, chips) * 2 + core
        return pltpu.make_async_remote_copy(
            src_ref=res.at[c],
            dst_ref=buf.at[c, core, z],
            send_sem=send_sem.at[c],
            recv_sem=direct_sem.at[c],
            device_id={"pp": lax.rem(stage + 1, stages), "tp": target},
            device_id_type=pl.DeviceIdType.MESH,
        )

    def to_out(c):
        return pltpu.make_async_remote_copy(
            src_ref=res.at[c],
            dst_ref=out_ref,
            send_sem=send_sem.at[c],
            recv_sem=out_sem,
            device_id={"pp": c, "tp": lane},
            device_id_type=pl.DeviceIdType.MESH,
        )

    def step(c, carry):
        whole_wait(c, core, direct_sem.at[c])
        forward(c).start()
        whole_wait(c, 1 - core, forward_sem.at[c])

        current = jnp.concatenate(
            [buf[c, k % 2, k // 2] for k in range(lanes_axis)], axis=1
        ).astype(F32)
        inverse = lax.rsqrt(
            jnp.sum(current * current, axis=1, keepdims=True) / width + EPSILON
        )
        scaled = (current * gain).astype(BF16)
        projected = mm(scaled, weights[...], NT) * inverse
        query_pre = projected[:, 0 * cols : 1 * cols]
        forget_pre = projected[:, 1 * cols : 2 * cols]
        values = projected[:, 2 * cols : 3 * cols].astype(BF16)
        gate_pre = projected[:, 3 * cols : 4 * cols]

        key_in = span * sigmoid(-forget_pre)
        log_forget = jnp.log(1.0 - key_in) + spikes[lax.rem(c, 2)]
        high = log_forget.astype(BF16)
        low = (log_forget - high.astype(F32)).astype(BF16)
        running = mm(tril_ones, high, NN) + mm(tril_ones, low, NN)
        ending = running[rows - 1 : rows, :]
        query_scaled = query_pre * sigmoid(query_pre) * jnp.exp(running)
        key_scaled = (key_in * jnp.exp(-running)).astype(BF16)
        key_end = (key_in * jnp.exp(ending - running)).astype(BF16)
        query_bf = query_scaled.astype(BF16)
        tall_query = jnp.concatenate(
            [jnp.where(head_of_lane == h, query_scaled, 0.0).astype(BF16) for h in range(heads)],
            axis=0,
        )
        scores = jnp.where(tall_mask, mm(tall_query, key_scaled, NT), 0.0).astype(BF16)
        tall_mixed = mm(scores, values, NN)
        memory = jnp.where(lax.rem(c, 2) == 0, 0.0, state[...])
        mixed = mm(query_bf, memory.astype(BF16), NT)
        inner = tall_mixed[0:rows]
        for h in range(1, heads):
            inner = jnp.where(head_of_lane == h, tall_mixed[h * rows : (h + 1) * rows], inner)
        mixed = mixed + inner
        mean_square = mm((mixed * mixed).astype(BF16), mean_ones, NN)
        branch = mixed * lax.rsqrt(mean_square + EPSILON) * out_gain
        branch = branch * (gate_pre * sigmoid(gate_pre))
        res[c] = (buf[c, core, z].astype(F32) + branch).astype(BF16)

        @pl.when(stage != stages - 1)
        def _():
            for far in range(chips):
                to_next(c, far).start()

        @pl.when((stage == stages - 1) & (c != stage))
        def _():
            to_out(c).start()

        @pl.when((stage == stages - 1) & (c == stage))
        def _():
            pltpu.make_async_copy(res.at[c], out_ref, out_sem).start()

        added = jnp.where(same_head, mm(values, key_end, TN), 0.0)
        state[...] = memory * jnp.exp(ending) + added
        return carry

    lax.fori_loop(0, chunks, step, 0)

    for far in range(1, chips):
        to_first(far).wait_send()

    @pl.when(stage != 0)
    def _():
        to_first(0).wait_send()

    def drain(c, carry):
        forward(c).wait_send()

        @pl.when(stage != stages - 1)
        def _():
            whole_wait(c, core, send_sem.at[c])

        @pl.when((stage == stages - 1) & (c != stage))
        def _():
            to_out(c).wait_send()

        return carry

    lax.fori_loop(0, chunks, drain, 0)
    pltpu.make_async_copy(out_ref, out_ref, out_sem).wait()


def solution(mesh):
    stages = mesh.shape["pp"]
    lanes_axis = mesh.shape["tp"]
    chips = lanes_axis // 2

    def step(x, gain, wq, wf, wi, wg, low, spike, scale):
        rows, cols = x.shape
        width = gain.shape[1]
        vmem = pl.BlockSpec(memory_space=pltpu.VMEM)
        hbm = pl.BlockSpec(memory_space=pl.ANY)
        dma = pltpu.SemaphoreType.DMA
        return pl.pallas_call(
            functools.partial(kernel, stages, lanes_axis),
            out_shape=jax.ShapeDtypeStruct((rows, cols), BF16),
            in_specs=[vmem, vmem, hbm, hbm, hbm, hbm, vmem, vmem, vmem],
            out_specs=vmem,
            scratch_shapes=[
                pltpu.VMEM((4 * cols, width), BF16),
                pltpu.VMEM((stages, 2, chips, rows, cols), BF16),
                pltpu.VMEM((stages, rows, cols), BF16),
                pltpu.VMEM((2, rows, cols), F32),
                pltpu.VMEM((cols, cols), F32),
                dma((4,)),
                dma((chips,)),
                dma,
                dma((stages,)),
                dma((stages,)),
                dma((stages,)),
                dma((stages,)),
                dma,
            ],
            compiler_params=pltpu.CompilerParams(
                has_side_effects=True, vmem_limit_bytes=67043328
            ),
        )(x, gain, wq, wf, wi, wg, low, spike.transpose(0, 2, 1), scale)

    in_specs = (
        P("pp", "tp"),
        P("pp", None),
        P("pp", "tp", None),
        P("pp", "tp", None),
        P("pp", "tp", None),
        P("pp", "tp", None),
        P("pp", "tp"),
        P("pp", None, "tp"),
        P("pp", None),
    )
    return jax.shard_map(
        step, mesh=mesh, in_specs=in_specs, out_specs=P("pp", "tp"), check_vma=False
    )
```

time: 246 us -> 52 us (0.21); the launches traced: 242 us -> 51.7 us
  blocking collectives: 85.7 us -> 0 us
  waiting for transfers between devices: 67.1 us -> 0 us
  Pallas kernels: 0 us -> 50.3 us
  matrix products: 34.7 us -> 0 us
  local copies, waits for them, and re-layouts: 20.5 us -> 1.38 us
  between operations: 13.4 us -> 0.01 us
  other arithmetic: 12.1 us -> 0 us
  starting transfers between devices: 6.46 us -> 0 us
    all_gather x6 -> x0, blocking collectives: 85.7 us -> none  [the longest x5 79.7 us: one_step(): lax.all_gather(current, 'tp', axis=1, tiled=True)]
    pallas_call x0 -> x1, Pallas kernels: none -> 50.3 us  [step(): pl.pallas_call(functools.partial(kernel, stages, lanes_axis), out_shape=j...]
    psum x1 -> x0, waiting for transfers between devices: 43.4 us -> none  [spread(): return lax.psum(kept, axis)]
    dot_general x45 -> x0, matrix products: 34.7 us -> none  [the longest x5 20.8 us: add_piece(): lax.dot_general(scaled, weights, (((1,), (1,)), ((), ())), preferred_elem...]
    ppermute x5 -> x0, waiting for transfers between devices: 23.8 us -> none  [shifted(): return lax.ppermute(array, axis, pairs)]
    dynamic_slice x61 -> x0, local copies, waits for them, and re-layouts: 10.3 us -> none  [the longest x50 8.32 us: segment_scan(): lax.scan(one_block, memory, (split_blocks(queries), split_blocks(key_in),...]
    ppermute x5 -> x0, starting transfers between devices: 6.46 us -> none  [shifted(): return lax.ppermute(array, axis, pairs)]
    reshape x25 -> x0, local copies, waits for them, and re-layouts: 4.72 us -> none  [the longest x20 3.79 us: split_blocks(): tensor.reshape(head_count, blocks_count, SEG, tensor.shape[-1])]
  transfers between devices with their start and end apart: 6 -> 0, of which waited for: 6 -> 0; matrix products, arithmetic and copies ran while one was open for 0% -> 0% of each run, Pallas kernels for 0% -> 0%
where the time goes in v1:
time: 52 us; the launch traced here: 51.7 us
  Pallas kernels  50.3 us (97%)
  local copies, waits for them, and re-layouts  1.38 us (3%)
    pallas_call x1, Pallas kernels, step(): pl.pallas_call(functools.partial(kernel, stages, lanes_axis), out_shape=j...  50.3 us
    unnamed x1, local copies, waits for them, and re-layouts  1.38 us

profile of v1, /device:TPU:7, one launch (start us, length us, event | category | flops | bytes accessed | tf_op | source)
XLA Modules:
  0.0 51.7 jit_solution(5668840526716653241)
XLA Ops:
  0.0 50.3 %shard_map.91 = bf16[64,256]{1,0:T(8,128)(2,1)} custom-call(bf16[64,256]{1,0:T(8,128)(2,1)} %x_ref.1, f32[1,2048]{1,0:T(1,128)} %gain_ref.1, bf16[1,256,2048]{2,1,0:T(8,128)(2,1)} %wq_ref.1, bf16[1,256,2048]{2,1,0:T(8,128)(2,1)} %wf_ref.1, bf16[1,256,2048]{2,1,0:T(8,128)(2,1)} %wi_ref.1, bf16[1,256,2048]{2,1,0:T(8,128)(2,1)} %wg_ref.1, f32[1,256]{1,0:T(1,128)} %low_ref.1, ...), custom_call_target="tpu_custom_call" | custom-call | tf_op jit(solution)/shard_map/pallas_call | solution.py:257
  50.3 1.4 %copy.11 = bf16[64,256]{1,0:T(8,128)(2,1)} copy(bf16[64,256]{1,0:T(8,128)(2,1)} %shard_map.91) | data formatting | bytes 65536

commit v2 on v1

--- a/solution.py
+++ b/solution.py
@@ -22,6 +22,15 @@
 
 def sigmoid(v):
     return 1.0 / (1.0 + jnp.exp(-v))
+
+
+def signal_to(semaphore, stage, lane):
+    pl.semaphore_signal(
+        semaphore,
+        inc=1,
+        device_id={"pp": stage, "tp": lane},
+        device_id_type=pl.DeviceIdType.MESH,
+    )
 
 
 def kernel(
@@ -44,7 +53,6 @@
     state,
     w_sem,
     in_send,
-    local_sem,
     direct_sem,
     forward_sem,
     send_sem,
@@ -70,28 +78,48 @@
         load.start()
         loads.append(load)
 
-    def to_first(far):
-        target = lax.rem(z + far, chips) * 2 + core
+    barrier = pltpu.get_barrier_semaphore()
+    for up in range(stages):
+        for over in range(chips):
+            if up or over:
+                signal_to(
+                    barrier,
+                    lax.rem(stage + up, stages),
+                    lax.rem(z + over, chips) * 2 + core,
+                )
+    signal_to(barrier, stage, partner)
+    pl.semaphore_wait(barrier, stages * chips)
+
+    def farthest_first(send):
+        for far in range(chips - 1, 0, -1):
+
+            @pl.when(z + far < chips)
+            def _():
+                send(z + far)
+
+            @pl.when(z - far >= 0)
+            def _():
+                send(z - far)
+
+    def to_first(target):
         return pltpu.make_async_remote_copy(
             src_ref=x_ref,
             dst_ref=buf.at[stage, core, z],
-            send_sem=in_send.at[far],
+            send_sem=in_send.at[target],
             recv_sem=direct_sem.at[stage],
-            device_id={"pp": 0, "tp": target},
+            device_id={"pp": 0, "tp": target * 2 + core},
             device_id_type=pl.DeviceIdType.MESH,
         )
 
-    own_copy = pltpu.make_async_copy(x_ref, buf.at[stage, core, z], direct_sem.at[stage])
-    for far in range(1, chips):
-        to_first(far).start()
+    farthest_first(lambda target: to_first(target).start())
 
     @pl.when(stage != 0)
     def _():
-        to_first(0).start()
+        to_first(z).start()
 
     @pl.when(stage == 0)
     def _():
-        own_copy.start()
+        pltpu.make_async_copy(x_ref, buf.at[stage, core, z], direct_sem.at[stage]).start()
 
     head_of_lane = lax.broadcasted_iota(jnp.int32, (rows, cols), 1) // HEAD
     for part in range(2):
@@ -112,8 +140,7 @@
     sq_col = lax.broadcasted_iota(jnp.int32, (cols, cols), 1) // HEAD
     same_head = sq_row == sq_col
     mean_ones = jnp.where(same_head, 1.0 / HEAD, 0.0).astype(BF16)
-    gain = gain_ref[...]
-    span = 1.0 - low_ref[...]
+    keep_span = 1.0 - low_ref[...]
     out_gain = jnp.concatenate([scale_ref[...]] * heads, axis=1)
 
     for load in loads:
@@ -134,14 +161,13 @@
             device_id_type=pl.DeviceIdType.MESH,
         )
 
-    def to_next(c, far):
-        target = lax.rem(z + far, chips) * 2 + core
+    def to_next(c, target):
         return pltpu.make_async_remote_copy(
             src_ref=res.at[c],
             dst_ref=buf.at[c, core, z],
             send_sem=send_sem.at[c],
             recv_sem=direct_sem.at[c],
-            device_id={"pp": lax.rem(stage + 1, stages), "tp": target},
+            device_id={"pp": lax.rem(stage + 1, stages), "tp": target * 2 + core},
             device_id_type=pl.DeviceIdType.MESH,
         )
 
@@ -155,25 +181,40 @@
             device_id_type=pl.DeviceIdType.MESH,
         )
 
+    def half_product(c, which):
+        spans = [
+            pl.ds(pl.multiple_of((2 * k + which) * cols, cols), cols) for k in range(chips)
+        ]
+        current = jnp.concatenate([buf[c, which, k] for k in range(chips)], axis=1).astype(F32)
+        gain = jnp.concatenate([gain_ref[:, span] for span in spans], axis=1)
+        matrix = jnp.concatenate([weights[:, span] for span in spans], axis=1)
+        product = mm((current * gain).astype(BF16), matrix, NT)
+        return product, jnp.sum(current * current, axis=1, keepdims=True)
+
     def step(c, carry):
         whole_wait(c, core, direct_sem.at[c])
         forward(c).start()
-        whole_wait(c, 1 - core, forward_sem.at[c])
-
-        current = jnp.concatenate(
-            [buf[c, k % 2, k // 2] for k in range(lanes_axis)], axis=1
-        ).astype(F32)
-        inverse = lax.rsqrt(
-            jnp.sum(current * current, axis=1, keepdims=True) / width + EPSILON
-        )
-        scaled = (current * gain).astype(BF16)
-        projected = mm(scaled, weights[...], NT) * inverse
+
+        if cols % 128 == 0:
+            first, first_sum = half_product(c, core)
+            whole_wait(c, 1 - core, forward_sem.at[c])
+            second, second_sum = half_product(c, 1 - core)
+            product, squares = first + second, first_sum + second_sum
+        else:
+            whole_wait(c, 1 - core, forward_sem.at[c])
+            current = jnp.concatenate(
+                [buf[c, k % 2, k // 2] for k in range(lanes_axis)], axis=1
+            ).astype(F32)
+            squares = jnp.sum(current * current, axis=1, keepdims=True)
+            scaled = (current * gain_ref[...]).astype(BF16)
+            product = mm(scaled, weights[...], NT)
+        projected = product * lax.rsqrt(squares / width + EPSILON)
         query_pre = projected[:, 0 * cols : 1 * cols]
         forget_pre = projected[:, 1 * cols : 2 * cols]
         values = projected[:, 2 * cols : 3 * cols].astype(BF16)
         gate_pre = projected[:, 3 * cols : 4 * cols]
 
-        key_in = span * sigmoid(-forget_pre)
+        key_in = keep_span * sigmoid(-forget_pre)
         log_forget = jnp.log(1.0 - key_in) + spikes[lax.rem(c, 2)]
         high = log_forget.astype(BF16)
         low = (log_forget - high.astype(F32)).astype(BF16)
@@ -202,8 +243,8 @@
 
         @pl.when(stage != stages - 1)
         def _():
-            for far in range(chips):
-                to_next(c, far).start()
+            farthest_first(lambda target: to_next(c, target).start())
+            to_next(c, z).start()
 
         @pl.when((stage == stages - 1) & (c != stage))
         def _():
@@ -219,12 +260,11 @@
 
     lax.fori_loop(0, chunks, step, 0)
 
-    for far in range(1, chips):
-        to_first(far).wait_send()
+    farthest_first(lambda target: to_first(target).wait_send())
 
     @pl.when(stage != 0)
     def _():
-        to_first(0).wait_send()
+        to_first(z).wait_send()
 
     def drain(c, carry):
         forward(c).wait_send()
@@ -267,7 +307,6 @@
                 pltpu.VMEM((cols, cols), F32),
                 dma((4,)),
                 dma((chips,)),
-                dma,
                 dma((stages,)),
                 dma((stages,)),
                 dma((stages,)),
@@ -275,7 +314,7 @@
                 dma,
             ],
             compiler_params=pltpu.CompilerParams(
-                has_side_effects=True, vmem_limit_bytes=67043328
+                collective_id=0, has_side_effects=True, vmem_limit_bytes=67043328
             ),
         )(x, gain, wq, wf, wi, wg, low, spike.transpose(0, 2, 1), scale)
 

time: 52 us -> 50.4 us (0.969)
  Pallas kernels: 50.3 us -> 48.8 us
    pallas_call x1, Pallas kernels: 50.3 us -> 48.8 us  [step(): pl.pallas_call(functools.partial(kernel, stages, lanes_axis), out_shape=j...]
where the time goes in v2:
time: 50.4 us; the launch traced here: 50.2 us
  Pallas kernels  48.8 us (97%)
  local copies, waits for them, and re-layouts  1.38 us (3%)
    pallas_call x1, Pallas kernels, step(): pl.pallas_call(functools.partial(kernel, stages, lanes_axis), out_shape=j...  48.8 us
    unnamed x1, local copies, waits for them, and re-layouts  1.38 us

profile of v2, /device:TPU:7, one launch (start us, length us, event | category | flops | bytes accessed | tf_op | source)
XLA Modules:
  0.0 50.2 jit_solution(1557517992799856436)
XLA Ops:
  0.0 48.8 %shard_map.91 = bf16[64,256]{1,0:T(8,128)(2,1)} custom-call(bf16[64,256]{1,0:T(8,128)(2,1)} %x_ref.1, f32[1,2048]{1,0:T(1,128)} %gain_ref.1, bf16[1,256,2048]{2,1,0:T(8,128)(2,1)} %wq_ref.1, bf16[1,256,2048]{2,1,0:T(8,128)(2,1)} %wf_ref.1, bf16[1,256,2048]{2,1,0:T(8,128)(2,1)} %wi_ref.1, bf16[1,256,2048]{2,1,0:T(8,128)(2,1)} %wg_ref.1, f32[1,256]{1,0:T(1,128)} %low_ref.1, ...), custom_call_target="tpu_custom_call" | custom-call | tf_op jit(solution)/shard_map/pallas_call | solution.py:297
  48.8 1.4 %copy.11 = bf16[64,256]{1,0:T(8,128)(2,1)} copy(bf16[64,256]{1,0:T(8,128)(2,1)} %shard_map.91) | data formatting | bytes 65536

commit v3 on v2

--- a/solution.py
+++ b/solution.py
@@ -8,6 +8,7 @@
 from jax.sharding import PartitionSpec as P
 
 HEAD = 64
+TILE = 256
 EPSILON = 1e-06
 F32 = jnp.float32
 BF16 = jnp.bfloat16
@@ -47,6 +48,7 @@
     scale_ref,
     out_ref,
     weights,
+    turned,
     buf,
     res,
     spikes,
@@ -143,8 +145,17 @@
     keep_span = 1.0 - low_ref[...]
     out_gain = jnp.concatenate([scale_ref[...]] * heads, axis=1)
 
-    for load in loads:
+    for role, load in enumerate(loads):
         load.wait()
+
+        def turn(k, carry, role=role):
+            tile = pl.ds(pl.multiple_of(k * TILE, TILE), TILE)
+            turned[tile, role * cols : (role + 1) * cols] = weights[
+                role * cols : (role + 1) * cols, tile
+            ].T
+            return carry
+
+        lax.fori_loop(0, width // TILE, turn, 0)
 
     def whole_wait(c, which, sem):
         half = buf.at[c, which]
@@ -181,33 +192,17 @@
             device_id_type=pl.DeviceIdType.MESH,
         )
 
-    def half_product(c, which):
-        spans = [
-            pl.ds(pl.multiple_of((2 * k + which) * cols, cols), cols) for k in range(chips)
-        ]
-        current = jnp.concatenate([buf[c, which, k] for k in range(chips)], axis=1).astype(F32)
-        gain = jnp.concatenate([gain_ref[:, span] for span in spans], axis=1)
-        matrix = jnp.concatenate([weights[:, span] for span in spans], axis=1)
-        product = mm((current * gain).astype(BF16), matrix, NT)
-        return product, jnp.sum(current * current, axis=1, keepdims=True)
-
     def step(c, carry):
         whole_wait(c, core, direct_sem.at[c])
         forward(c).start()
 
-        if cols % 128 == 0:
-            first, first_sum = half_product(c, core)
-            whole_wait(c, 1 - core, forward_sem.at[c])
-            second, second_sum = half_product(c, 1 - core)
-            product, squares = first + second, first_sum + second_sum
-        else:
-            whole_wait(c, 1 - core, forward_sem.at[c])
-            current = jnp.concatenate(
-                [buf[c, k % 2, k // 2] for k in range(lanes_axis)], axis=1
-            ).astype(F32)
-            squares = jnp.sum(current * current, axis=1, keepdims=True)
-            scaled = (current * gain_ref[...]).astype(BF16)
-            product = mm(scaled, weights[...], NT)
+        whole_wait(c, 1 - core, forward_sem.at[c])
+        current = jnp.concatenate(
+            [buf[c, k % 2, k // 2] for k in range(lanes_axis)], axis=1
+        ).astype(F32)
+        squares = jnp.sum(current * current, axis=1, keepdims=True)
+        scaled = (current * gain_ref[...]).astype(BF16)
+        product = mm(scaled, turned[...], NN)
         projected = product * lax.rsqrt(squares / width + EPSILON)
         query_pre = projected[:, 0 * cols : 1 * cols]
         forget_pre = projected[:, 1 * cols : 2 * cols]
@@ -301,6 +296,7 @@
             out_specs=vmem,
             scratch_shapes=[
                 pltpu.VMEM((4 * cols, width), BF16),
+                pltpu.VMEM((width, 4 * cols), BF16),
                 pltpu.VMEM((stages, 2, chips, rows, cols), BF16),
                 pltpu.VMEM((stages, rows, cols), BF16),
                 pltpu.VMEM((2, rows, cols), F32),

time: 50.4 us -> 46.9 us (0.931)
  Pallas kernels: 48.8 us -> 45.2 us
    pallas_call x1, Pallas kernels: 48.8 us -> 45.2 us  [step(): pl.pallas_call(functools.partial(kernel, stages, lanes_axis), out_shape=j...]
where the time goes in v3:
time: 46.9 us; the launch traced here: 46.6 us
  Pallas kernels  45.2 us (96%)
  local copies, waits for them, and re-layouts  1.38 us (3%)
    pallas_call x1, Pallas kernels, step(): pl.pallas_call(functools.partial(kernel, stages, lanes_axis), out_shape=j...  45.2 us
    unnamed x1, local copies, waits for them, and re-layouts  1.38 us

profile of v3, /device:TPU:7, one launch (start us, length us, event | category | flops | bytes accessed | tf_op | source)
XLA Modules:
  0.0 46.6 jit_solution(1681539567043064044)
XLA Ops:
  0.0 45.2 %shard_map.91 = bf16[64,256]{1,0:T(8,128)(2,1)} custom-call(bf16[64,256]{1,0:T(8,128)(2,1)} %x_ref.1, f32[1,2048]{1,0:T(1,128)} %gain_ref.1, bf16[1,256,2048]{2,1,0:T(8,128)(2,1)} %wq_ref.1, bf16[1,256,2048]{2,1,0:T(8,128)(2,1)} %wf_ref.1, bf16[1,256,2048]{2,1,0:T(8,128)(2,1)} %wi_ref.1, bf16[1,256,2048]{2,1,0:T(8,128)(2,1)} %wg_ref.1, f32[1,256]{1,0:T(1,128)} %low_ref.1, ...), custom_call_target="tpu_custom_call" | custom-call | tf_op jit(solution)/shard_map/pallas_call | solution.py:292
  45.2 1.4 %copy.11 = bf16[64,256]{1,0:T(8,128)(2,1)} copy(bf16[64,256]{1,0:T(8,128)(2,1)} %shard_map.91) | data formatting | bytes 65536
